TPU v7x, 512 devices: a whole 4x4x16 slice. The times are simulated.
512 devices in a mesh: sp: 64 (over z, y), dp: 8 (over x, core).
Axes of the slice: x: 4, y: 4, z: 16, core: 2. Of those that a mesh axis runs over, the one named last changes fastest.
Arguments:
- val_input: bfloat16 [8192, 1536], P('sp', 'dp'), may hold values from -24 to 24, as said below
- gate_input: bfloat16 [8192, 1536], P('sp', 'dp'), may hold values from -8 to 8
- cotangent: bfloat16 [8192, 4096], P('sp'), may hold values from -16 to 16
- out_weight: bfloat16 [4096, 1536], P('sp', 'dp'), may hold values from -0.09375 to 0.09375
- conv_taps: float32 [31, 1536], P(None, 'dp'), may hold values from -1 to 1
- norm_gain: float32 [1536], P('dp'), may hold values from 0.1 to 1.9
Outputs:
- grad_val: bfloat16 [8192, 1536], P('sp', 'dp')
- grad_gate: bfloat16 [8192, 1536], P('sp', 'dp')
- grad_out_weight: float32 [4096, 1536], P('sp', 'dp')
- grad_taps: float32 [31, 1536], P(None, 'dp')
- grad_gain: float32 [1536], P('dp')
Inputs may be any that keep to these rules, and one draw needn't show every extreme that they name: `val_input`: blocks of 64 channels and blocks of 32 tokens carry their own scales.
All inputs are finite; a program needn't handle non-finite values.
Results may differ from a plain program's by a relative error of at most 0.0063.
Values may be sent and summed in bfloat16 or wider, within the bound.
No kernel may reach another device: no remote copies, remote signals or barrier semaphores. Data moves between devices by JAX's collectives and lax.ppermute only.
A program may use at most 64 MiB of HBM per device.

v0:
```python
import jax
import jax.numpy as jnp
from jax import lax
from jax.sharding import Mesh
from jax.sharding import PartitionSpec as P

SP = ("sp_0", "sp_1")


norm_floor = 0.25


def whole_of(array, axes, dim):
    if not axes:
        return array
    nearer = lax.all_gather(array, axes[-1], axis=dim, tiled=True)
    return whole_of(nearer, axes[:-1], dim)


def passed_along(value, axis, steps):
    count = lax.axis_size(axis)
    first, last = (max(0, -steps), min(count, count - steps))
    return lax.ppermute(value, axis, [(source, source + steps) for source in range(first, last)])


def from_everyone(array, axis):
    copies = jnp.broadcast_to(array, (lax.axis_size(axis), *array.shape))
    return lax.all_to_all(copies, axis, split_axis=0, concat_axis=0, tiled=True)


def taken_together(array, axis):
    return from_everyone(array, axis).sum(axis=0)


def packed_total(arrays, axis):
    ravelled, at, finished = (jnp.concatenate([a.reshape(-1) for a in arrays]), 0, [])
    running = taken_together(ravelled, axis)
    for a in arrays:
        finished.append(running[at : at + a.size].reshape(a.shape))
        at += a.size
    return tuple(finished)


def own_block(blocks, axes, turns):
    lengths = [lax.axis_size(a) for a in axes]
    blocks = blocks.reshape(*lengths, *blocks.shape[1:])
    blocks = blocks.transpose(*turns, *range(len(axes), blocks.ndim))
    blocks = blocks.reshape(-1, *blocks.shape[len(axes) :])
    for k in turns:
        blocks = lax.psum_scatter(blocks, axes[k], scatter_dimension=0, tiled=True)
    return blocks[0]


def split_up(array, dim, length):
    lengths = array.shape
    blocks = array.reshape(*lengths[:dim], length, lengths[dim] // length, *lengths[dim + 1 :])
    return jnp.moveaxis(blocks, dim, 0)


def scatter_axes(array, axes, turns, dim):
    length = lax.axis_size(axes)
    return own_block(split_up(array, dim, length), axes, turns)


def by_axis(array, axes):
    for axis in axes:
        array = lax.psum(array, axis)
    return array


def per_device(val_input, gate_input, cotangent, out_weight, conv_taps, norm_gain):
    rows_here = val_input.shape[0]
    width_dp = val_input.shape[1]
    taps = conv_taps.shape[0]
    channels = width_dp * lax.axis_size("dp")
    columns = cotangent
    grad_mix = jnp.dot(columns, whole_of(out_weight, SP, 0), preferred_element_type=jnp.float32)
    sigma_gate = jax.nn.sigmoid(gate_input.astype(jnp.float32))
    mixed_in = (val_input.astype(jnp.float32) * sigma_gate).astype(jnp.bfloat16)
    earlier = passed_along(mixed_in[rows_here - (taps - 1) :], SP, 1)
    padded_in = jnp.concatenate([earlier, lax.optimization_barrier(mixed_in)], 0).astype(
        jnp.float32
    )
    conv_out = jnp.zeros((rows_here, width_dp), jnp.float32)
    for offset in range(taps):
        conv_out = conv_out + conv_taps[offset][None, :] * padded_in[offset : offset + rows_here]
    conv_rows = lax.optimization_barrier(conv_out.astype(jnp.bfloat16)).astype(jnp.float32)
    row_sums = packed_total((jnp.sum(conv_rows, 1), jnp.sum(conv_rows * conv_rows, 1)), "dp")
    row_mean = row_sums[0][:, None] / channels
    row_var = row_sums[1][:, None] / channels - row_mean * row_mean
    inv_scale = lax.rsqrt(row_var + norm_floor)
    normed = (conv_rows - row_mean) * inv_scale
    act = normed * norm_gain[None, :]
    sigma_act = jax.nn.sigmoid(act)
    swished = (act * sigma_act).astype(jnp.bfloat16)
    columns = cotangent
    grad_out_weight = scatter_axes(
        lax.dot_general(
            columns, swished, (((0,), (0,)), ((), ())), preferred_element_type=jnp.float32
        ),
        SP,
        (1, 0),
        0,
    )
    grad_act = grad_mix * sigma_act * (1.0 + act * (1.0 - sigma_act))
    gain_part = jnp.sum(grad_act * normed, 0)
    grad_norm = grad_act * norm_gain[None, :]
    norm_sums = packed_total((jnp.sum(grad_norm, 1), jnp.sum(grad_norm * normed, 1)), "dp")
    first_sum = norm_sums[0][:, None] / channels
    second_sum = norm_sums[1][:, None] / channels
    grad_conv = (inv_scale * (grad_norm - first_sum - normed * second_sum)).astype(jnp.bfloat16)
    later = passed_along(grad_conv[: taps - 1], SP, -1)
    padded_grad = jnp.concatenate([lax.optimization_barrier(grad_conv), later], 0).astype(
        jnp.float32
    )
    own_grad = padded_grad[:rows_here]
    grad_mixed = jnp.zeros((rows_here, width_dp), jnp.float32)
    tap_list = []
    for offset in range(taps):
        back = taps - 1 - offset
        grad_mixed = grad_mixed + conv_taps[offset][None, :] * padded_grad[back : back + rows_here]
        tap_list.append(jnp.sum(own_grad * padded_in[offset : offset + rows_here], 0))
    grad_taps, grad_gain = (by_axis(jnp.stack(tap_list, 0), SP), by_axis(gain_part, SP))
    grad_rows = lax.optimization_barrier(grad_mixed.astype(jnp.bfloat16)).astype(jnp.float32)
    grad_val = (grad_rows * sigma_gate).astype(jnp.bfloat16)
    grad_gate = (
        grad_rows * val_input.astype(jnp.float32) * sigma_gate * (1.0 - sigma_gate)
    ).astype(jnp.bfloat16)
    return (grad_val, grad_gate, grad_out_weight, grad_taps, grad_gain)


def solution(mesh):
    split = Mesh(mesh.devices.reshape(16, 4, mesh.shape["dp"]), ("sp_0", "sp_1", "dp"))
    in_specs = (P(SP, "dp"), P(SP, "dp"), P(SP, None), P(SP, "dp"), P(None, "dp"), P("dp"))
    out_specs = (P(SP, "dp"), P(SP, "dp"), P(SP, "dp"), P(None, "dp"), P("dp"))
    return jax.shard_map(
        per_device, mesh=split, in_specs=in_specs, out_specs=out_specs, check_vma=False
    )
```

profile of v0, /device:TPU:2, one launch (start us, length us, event | category | flops | bytes accessed | tf_op | source)
XLA Modules:
  0.0 214.0 jit_solution(13165765928091978181)
XLA Ops:
  8.0 0.0 copy-start
  8.0 0.0 copy-start.3
  8.0 0.0 all-gather.2.cloned.1.call-start
  8.1 14.2 %all_gather.6 = bf16[256,192]{1,0:T(8,128)(2,1)} all-gather(bf16[64,192]{1,0:T(8,128)(2,1)} %param.9), channel_id=1, replica_groups=mesh['sp_0'=16,'sp_1'=4,'dp'=8] {'sp_1'}, dimensions={0}, use_global_device_ids=true | all-gather | bytes 122880 | tf_op jit(solution)/shard_map/all_gather | solution.py:16
  22.3 0.0 all-gather.2.cloned.1.call-update
  22.3 0.0 reduce-scatter.3.cloned.1.call-start
  22.4 0.9 fusion.1
  23.2 0.1 slice.459
  23.3 2.6 %collective-permute-start = (bf16[30,192]{0,1:T(8,128)(2,1)S(1)}, bf16[30,192]{0,1:T(8,128)(2,1)S(1)}, u32[]{:S(2)}, u32[]{:S(2)}) collective-permute-start(bf16[30,192]{0,1:T(8,128)(2,1)S(1)} %slice.459), channel_id=1, source_target_pairs={{0,8},{8,16},{16,24},{24,32},{32,40},{40,48},{48,56},{56,64},{64,7... | collective-permute-start | bytes 34568 | tf_op jit(solution)/shard_map/ppermute | solution.py:23
  25.9 1.1 fusion.62
  27.0 1.0 fusion.63
  27.9 0.0 collective-permute-done
  28.0 0.1 maximum_convert_fusion
  28.1 1.8 add_convert_fusion
  29.9 10.4 %all_to_all.12 = f32[8,1,256]{2,1,0:T(1,128)S(1)} all-to-all(f32[8,1,256]{2,1,0:T(1,128)S(1)} %broadcast_in_dim.4), channel_id=1, replica_groups=mesh['sp_0'=16,'sp_1'=4,'dp'=8] {'dp'}, dimensions={0} | all-to-all | bytes 16384 | tf_op jit(solution)/shard_map/all_to_all | solution.py:28
  40.4 0.0 copy-done
  40.4 0.0 copy-done.3
  40.4 2.3 %convolution_bitcast_fusion = f32[4096,192]{0,1:T(8,128)} fusion(bf16[128,4096]{1,0:T(8,128)(2,1)S(1)} %copy-done, bf16[128,192]{0,1:T(8,128)(2,1)S(1)} %add_convert_fusion, f32[192]{0:T(256)S(1)} %copy-done.3, f32[128]{0:T(128)S(1)} %get-tuple-element.85, f32[128]{0:T(128)S(1)} %get-tuple-element.84), kind=kOutput, calls=%fused_computation | convolution fusion | flops 201547776 | bytes 4245248 | tf_op jit(solution)/shard_map/dot_general | solution.py:98
  42.7 5.1 %copy.19 = f32[4096,192]{1,0:T(8,128)} copy(f32[4096,192]{0,1:T(8,128)} %convolution_bitcast_fusion) | data formatting | bytes 6291456 | tf_op jit(solution)/shard_map/dot_general | solution.py:98
  47.9 4.6 %copy.20 = f32[4,16,64,192]{3,2,1,0:T(8,128)} copy(f32[4,16,64,192]{3,2,0,1:T(8,128)} %bitcast.73) | data formatting | bytes 6291456 | tf_op jit(solution)/shard_map/transpose | solution.py:47
  52.5 0.0 reduce-scatter.3.cloned.1.call-update
  52.5 0.0 reduce-scatter.5.cloned.1.call-start
  52.6 45.5 %all-gather.2.cloned.1.call-done = bf16[4096,192]{1,0:T(8,128)(2,1)} async-done(((bf16[256,192]{1,0:T(8,128)(2,1)}), bf16[4096,192]{1,0:T(8,128)(2,1)}) %all-gather.2.cloned.1.call-update) | async-done | bytes 1572880 | tf_op jit(solution)/shard_map/all_gather | solution.py:16
  98.1 2.5 %fusion.24 = (f32[192]{0:T(256)S(1)}, f32[128]{0:T(128)S(1)}, f32[128]{0:T(128)S(1)}, f32[128,192]{0,1:T(8,128)S(1)}) fusion(bf16[128,192]{0,1:T(8,128)(2,1)S(1)} %add_convert_fusion, f32[128]{0:T(128)S(1)} %get-tuple-element.85, f32[128]{0:T(128)S(1)} %get-tuple-element.84, f32[192]{0:T(256)S(1)} %copy-done.3, bf16[128,4096]{1,0:T(8,128)(2,1)S(1)} %copy-done, ...), kind=kOutput, calls=%fused_computation.32 | convolution fusion | flops 201768512 | bytes 2772480 | tf_op jit(solution)/shard_map/dot_general | solution.py:77
  100.6 10.0 %reduce-scatter.3.cloned.1.call-done = f32[16,64,192]{2,1,0:T(8,128)} async-done(((f32[64,64,192]{2,1,0:T(8,128)}), f32[16,64,192]{2,1,0:T(8,128)}) %reduce-scatter.3.cloned.1.call-update) | async-done | bytes 786448 | tf_op jit(solution)/shard_map/reduce_scatter | solution.py:50
  110.7 0.0 reduce-scatter.5.cloned.1.call-update
  110.7 8.5 %all_to_all.13 = f32[8,1,256]{2,1,0:T(1,128)S(1)} all-to-all(f32[8,1,256]{2,1,0:T(1,128)S(1)} %broadcast_in_dim.5), channel_id=1, replica_groups=mesh['sp_0'=16,'sp_1'=4,'dp'=8] {'dp'}, dimensions={0} | all-to-all | bytes 16384 | tf_op jit(solution)/shard_map/all_to_all | solution.py:28
  119.2 0.1 fusion.23
  119.3 1.3 collective-permute-start.1
  120.6 4.7 %collective-permute-done.1 = bf16[30,192]{0,1:T(8,128)(2,1)S(1)} collective-permute-done((bf16[30,192]{0,1:T(8,128)(2,1)S(1)}, bf16[30,192]{0,1:T(8,128)(2,1)S(1)}, u32[]{:S(2)}, u32[]{:S(2)}) %collective-permute-start.1) | collective-permute-done | bytes 11552 | tf_op jit(solution)/shard_map/ppermute | solution.py:23
  125.3 0.0 copy-start.1
  125.4 0.0 copy-start.2
  125.4 1.8 fusion.27
  127.2 0.7 multiply_reduce_fusion.18
  127.9 0.7 multiply_reduce_fusion.9
  128.5 0.9 multiply_reduce_fusion
  129.4 0.1 stack.127
  129.5 57.1 %all-reduce = (f32[31,192]{1,0:T(8,128)S(1)}, f32[192]{0:T(256)S(1)}) all-reduce(f32[31,192]{1,0:T(8,128)S(1)} %stack.127, f32[192]{0:T(256)S(1)} %get-tuple-element.36), channel_id=1, replica_groups=mesh['sp_0'=16,'sp_1'=4,'dp'=8] {'sp_0'}, use_global_device_ids=true, to_apply=%region_39.0 | all-reduce | flops 6144 | bytes 49152 | tf_op jit(solution)/shard_map/psum | solution.py:67
  186.6 19.2 %all-reduce.1 = (f32[31,192]{1,0:T(8,128)}, f32[192]{0:T(256)}) all-reduce(f32[31,192]{1,0:T(8,128)S(1)} %get-tuple-element.41, f32[192]{0:T(256)S(1)} %get-tuple-element.42), channel_id=1, replica_groups=mesh['sp_0'=16,'sp_1'=4,'dp'=8] {'sp_1'}, use_global_device_ids=true, to_apply=%region_40.0 | all-reduce | flops 6144 | bytes 49152 | tf_op jit(solution)/shard_map/psum | solution.py:67
  205.8 0.0 copy-done.1
  205.8 0.0 copy-done.2
  205.8 0.7 fusion.5
  206.5 0.0 reduce-scatter.5.cloned.1.call-done
  (10 shorter events, 0.2 us)
Async XLA Ops:
  8.0 32.4 %copy-start = (bf16[128,4096]{1,0:T(8,128)(2,1)S(1)}, bf16[128,4096]{1,0:T(8,128)(2,1)}, u32[]{:S(2)}) copy-start(bf16[128,4096]{1,0:T(8,128)(2,1)} %param.8) | copy-start | bytes 3145732
  8.0 32.4 %copy-start.3 = (f32[192]{0:T(256)S(1)}, f32[192]{0:T(256)}, u32[]{:S(2)}) copy-start(f32[192]{0:T(256)} %param.11) | copy-start | bytes 2308
  8.0 90.1 %all-gather.2.cloned.1.call-start = ((), (), s32[]{:S(2)}) async-start(), calls=%async_computation.4 | async-start | bytes 2228224 | tf_op jit(solution)/shard_map/all_gather | solution.py:16
  22.3 88.4 %reduce-scatter.3.cloned.1.call-start = ((), (), s32[]{:S(2)}) async-start(), calls=%async_computation.5 | async-start | bytes 5242880 | tf_op jit(solution)/shard_map/reduce_scatter | solution.py:50
  23.3 4.6 %collective-permute-start = (bf16[30,192]{0,1:T(8,128)(2,1)S(1)}, bf16[30,192]{0,1:T(8,128)(2,1)S(1)}, u32[]{:S(2)}, u32[]{:S(2)}) collective-permute-start(bf16[30,192]{0,1:T(8,128)(2,1)S(1)} %slice.459), channel_id=1, source_target_pairs={{0,8},{8,16},{16,24},{24,32},{32,40},{40,48},{48,56},{56,64},{64,7... | collective-permute-start | bytes 34568 | tf_op jit(solution)/shard_map/ppermute | solution.py:23
  52.5 154.0 %reduce-scatter.5.cloned.1.call-start = ((), (), s32[]{:S(2)}) async-start(), calls=%async_computation.6 | async-start | bytes 1114112 | tf_op jit(solution)/shard_map/reduce_scatter | solution.py:50
  119.3 6.0 %collective-permute-start.1 = (bf16[30,192]{0,1:T(8,128)(2,1)S(1)}, bf16[30,192]{0,1:T(8,128)(2,1)S(1)}, u32[]{:S(2)}, u32[]{:S(2)}) collective-permute-start(bf16[30,192]{0,1:T(8,128)(2,1)S(1)} %bitcast.75), channel_id=1, source_target_pairs={{8,0},{16,8},{24,16},{32,24},{40,32},{48,40},{56,48},{64,56},{72,6... | collective-permute-start | bytes 34568 | tf_op jit(solution)/shard_map/ppermute | solution.py:23
  125.3 80.5 %copy-start.1 = (bf16[128,192]{0,1:T(8,128)(2,1)S(1)}, bf16[128,192]{0,1:T(8,128)(2,1)}, u32[]{:S(2)}) copy-start(bf16[128,192]{0,1:T(8,128)(2,1)} %param.6) | copy-start | bytes 147460
  125.4 80.5 %copy-start.2 = (bf16[128,192]{0,1:T(8,128)(2,1)S(1)}, bf16[128,192]{0,1:T(8,128)(2,1)}, u32[]{:S(2)}) copy-start(bf16[128,192]{0,1:T(8,128)(2,1)} %param.7) | copy-start | bytes 147460
Sparse Core Ops, SparseCore 0:
  22.4 75.6 all-gather.1
  110.8 71.1 reduce-scatter.4
Sparse Core Ops, SparseCore 1:
  52.6 58.0 reduce-scatter.2
where the time goes:
time: 215 us; the launch traced here: 214 us
  blocking collectives  109 us (51%)
  waiting for transfers between devices  60.3 us (28%)
  between operations  15.6 us (7%)
  local copies, waits for them, and re-layouts  12 us (6%)
  other arithmetic  7.74 us (4%)
  matrix products  4.84 us (2%)
  starting transfers between devices  3.98 us (2%)
    psum x2, blocking collectives, by_axis(): array = lax.psum(array, axis)  76.3 us
    all_gather x1, waiting for transfers between devices, whole_of(): nearer = lax.all_gather(array, axes[-1], axis=dim, tiled=True)  45.5 us
    all_to_all x2, blocking collectives, from_everyone(): return lax.all_to_all(copies, axis, split_axis=0, concat_axis=0, tiled=True)  18.9 us
    all_gather x1, blocking collectives, whole_of(): nearer = lax.all_gather(array, axes[-1], axis=dim, tiled=True)  14.2 us
    reduce_scatter x2, waiting for transfers between devices, own_block(): blocks = lax.psum_scatter(blocks, axes[k], scatter_dimension=0, tiled=True)  10 us
    dot_general x1, local copies, waits for them, and re-layouts, per_device(): lax.dot_general(columns, swished, (((0,), (0,)), ((), ())), preferred_ele...  5.12 us
    ppermute x2, waiting for transfers between devices, passed_along(): lax.ppermute(value, axis, [(source, source + steps) for source in range(f...  4.69 us
    transpose x1, local copies, waits for them, and re-layouts, own_block(): blocks = blocks.transpose(*turns, *range(len(axes), blocks.ndim))  4.64 us
  transfers between devices with their start and end apart: 5, of which 3 were waited for; matrix products, arithmetic and copies ran while one was open for 11% of the time, Pallas kernels for 0%

commit v1 on v0

v1 whole, which is shorter than its diff:
```python
import jax
import jax.numpy as jnp
from jax import lax
from jax.sharding import Mesh
from jax.sharding import PartitionSpec as P

SP = ("sp_0", "sp_1")


norm_floor = 0.25


def passed_along(value, axis, steps):
    count = lax.axis_size(axis)
    first, last = (max(0, -steps), min(count, count - steps))
    return lax.ppermute(value, axis, [(source, source + steps) for source in range(first, last)])


def exchange(blocks, axis):
    return lax.all_to_all(blocks, axis, split_axis=0, concat_axis=0, tiled=True)


def from_everyone(array, axis):
    return exchange(jnp.broadcast_to(array, (lax.axis_size(axis), *array.shape)), axis)


def packed_total(arrays, axis):
    ravelled = jnp.concatenate([a.reshape(-1) for a in arrays])
    total = from_everyone(ravelled, axis).sum(axis=0)
    at, finished = 0, []
    for a in arrays:
        finished.append(total[at : at + a.size].reshape(a.shape))
        at += a.size
    return tuple(finished)


def dense(blocks):
    half = blocks.shape[-2] // 2
    rest = jnp.concatenate([blocks[..., :half, 128:], blocks[..., half:, 128:]], -1)
    return jnp.concatenate([blocks[..., :128], rest], -2)


def undense(blocks):
    rows = blocks.shape[-2] * 2 // 3
    rest = blocks[..., rows:, :]
    rest = jnp.concatenate([rest[..., :64], rest[..., 64:]], -2)
    return jnp.concatenate([blocks[..., :rows, :], rest], -1)


def per_device(val_input, gate_input, cotangent, out_weight, conv_taps, norm_gain):
    rows_here = val_input.shape[0]
    width_dp = val_input.shape[1]
    taps = conv_taps.shape[0]
    channels = width_dp * lax.axis_size("dp")
    z_size, y_size = (lax.axis_size("sp_0"), lax.axis_size("sp_1"))
    d_rows = out_weight.shape[0]

    weight = undense(from_everyone(dense(out_weight), "sp_0")).reshape(z_size * d_rows, width_dp)
    columns = cotangent.reshape(rows_here, z_size, y_size, d_rows).transpose(2, 0, 1, 3)
    columns = exchange(columns.reshape(y_size, rows_here, z_size * d_rows), "sp_1")
    columns = columns.reshape(y_size * rows_here, z_size * d_rows)

    sigma_gate = jax.nn.sigmoid(gate_input.astype(jnp.float32))
    mixed_in = (val_input.astype(jnp.float32) * sigma_gate).astype(jnp.bfloat16)
    earlier = passed_along(mixed_in[rows_here - (taps - 1) :], SP, 1)
    padded_in = jnp.concatenate([earlier, lax.optimization_barrier(mixed_in)], 0).astype(
        jnp.float32
    )
    conv_out = jnp.zeros((rows_here, width_dp), jnp.float32)
    for offset in range(taps):
        conv_out = conv_out + conv_taps[offset][None, :] * padded_in[offset : offset + rows_here]
    conv_rows = lax.optimization_barrier(conv_out.astype(jnp.bfloat16)).astype(jnp.float32)
    row_sums = packed_total((jnp.sum(conv_rows, 1), jnp.sum(conv_rows * conv_rows, 1)), "dp")
    row_mean = row_sums[0][:, None] / channels
    row_var = row_sums[1][:, None] / channels - row_mean * row_mean
    inv_scale = lax.rsqrt(row_var + norm_floor)
    normed = (conv_rows - row_mean) * inv_scale
    act = normed * norm_gain[None, :]
    sigma_act = jax.nn.sigmoid(act)
    swished = (act * sigma_act).astype(jnp.bfloat16)

    swished_y = from_everyone(swished, "sp_1").reshape(y_size * rows_here, width_dp)
    weight_part = lax.dot_general(
        columns, swished_y, (((0,), (0,)), ((), ())), preferred_element_type=jnp.float32
    )
    weight_part = weight_part.astype(jnp.bfloat16).reshape(z_size, d_rows, width_dp)
    weight_part = exchange(dense(weight_part), "sp_0").astype(jnp.float32)
    grad_out_weight = undense(weight_part.sum(axis=0))

    mix_part = jnp.dot(columns, weight, preferred_element_type=jnp.float32).astype(jnp.bfloat16)
    mix_part = exchange(mix_part.reshape(y_size, rows_here, width_dp), "sp_1")
    grad_mix = mix_part.astype(jnp.float32).sum(axis=0)

    grad_act = grad_mix * sigma_act * (1.0 + act * (1.0 - sigma_act))
    gain_part = jnp.sum(grad_act * normed, 0)
    grad_norm = grad_act * norm_gain[None, :]
    norm_sums = packed_total((jnp.sum(grad_norm, 1), jnp.sum(grad_norm * normed, 1)), "dp")
    first_sum = norm_sums[0][:, None] / channels
    second_sum = norm_sums[1][:, None] / channels
    grad_conv = (inv_scale * (grad_norm - first_sum - normed * second_sum)).astype(jnp.bfloat16)
    grad_conv = lax.optimization_barrier(grad_conv)
    own_grad = grad_conv.astype(jnp.float32)
    tap_list = []
    for offset in range(taps):
        tap_list.append(jnp.sum(own_grad * padded_in[offset : offset + rows_here], 0))
    tail = jnp.stack(tap_list + [gain_part], 0)
    tail = tail.reshape(y_size, (taps + 1) // y_size, width_dp)
    tail = exchange(tail, "sp_1").sum(axis=0).astype(jnp.bfloat16)
    tail = from_everyone(tail, "sp_0").astype(jnp.float32).sum(axis=0)
    tail = from_everyone(tail, "sp_1").reshape(taps + 1, width_dp)
    grad_taps, grad_gain = (tail[:taps], tail[taps])

    later = passed_along(grad_conv[: taps - 1], SP, -1)
    padded_grad = jnp.concatenate([grad_conv, later], 0).astype(jnp.float32)
    grad_mixed = jnp.zeros((rows_here, width_dp), jnp.float32)
    for offset in range(taps):
        back = taps - 1 - offset
        grad_mixed = grad_mixed + conv_taps[offset][None, :] * padded_grad[back : back + rows_here]
    grad_rows = lax.optimization_barrier(grad_mixed.astype(jnp.bfloat16)).astype(jnp.float32)
    grad_val = (grad_rows * sigma_gate).astype(jnp.bfloat16)
    grad_gate = (
        grad_rows * val_input.astype(jnp.float32) * sigma_gate * (1.0 - sigma_gate)
    ).astype(jnp.bfloat16)
    return (grad_val, grad_gate, grad_out_weight, grad_taps, grad_gain)


def solution(mesh):
    split = Mesh(mesh.devices.reshape(16, 4, mesh.shape["dp"]), ("sp_0", "sp_1", "dp"))
    in_specs = (P(SP, "dp"), P(SP, "dp"), P(SP, None), P(SP, "dp"), P(None, "dp"), P("dp"))
    out_specs = (P(SP, "dp"), P(SP, "dp"), P(SP, "dp"), P(None, "dp"), P("dp"))
    return jax.shard_map(
        per_device, mesh=split, in_specs=in_specs, out_specs=out_specs, check_vma=False
    )
```

time: 215 us -> 176 us (0.82)
  the two profiles are of different devices: /device:TPU:2 before, /device:TPU:64 now
where the time goes in v1:
time: 176 us; the launch traced here: 175 us
  waiting for transfers between devices  82 us (47%)
  starting transfers between devices  56.8 us (32%)
  blocking collectives  15.5 us (9%)
  other arithmetic  9.61 us (5%)
  local copies, waits for them, and re-layouts  8.76 us (5%)
    all_to_all x8, waiting for transfers between devices, exchange(): return lax.all_to_all(blocks, axis, split_axis=0, concat_axis=0, tiled=True)  68.8 us
    all_to_all x8, starting transfers between devices, exchange(): return lax.all_to_all(blocks, axis, split_axis=0, concat_axis=0, tiled=True)  50.3 us
    all_to_all x2, blocking collectives, exchange(): return lax.all_to_all(blocks, axis, split_axis=0, concat_axis=0, tiled=True)  15.5 us
    ppermute x2, waiting for transfers between devices, passed_along(): lax.ppermute(value, axis, [(source, source + steps) for source in range(f...  13.3 us
    ppermute x2, starting transfers between devices, passed_along(): lax.ppermute(value, axis, [(source, source + steps) for source in range(f...  6.54 us
  transfers between devices with their start and end apart: 10, of which 10 were waited for; matrix products, arithmetic and copies ran while one was open for 4% of the time, Pallas kernels for 0%

profile of v1, /device:TPU:64, one launch (start us, length us, event | category | flops | bytes accessed | tf_op | source)
XLA Modules:
  0.0 174.6 jit_solution(17569012560487640019)
XLA Ops:
  0.6 0.9 fusion.3
  1.6 3.5 %collective-permute-start = (bf16[30,192]{0,1:T(8,128)(2,1)S(1)}, bf16[30,192]{0,1:T(8,128)(2,1)S(1)}, u32[]{:S(2)}, u32[]{:S(2)}) collective-permute-start(bf16[30,192]{0,1:T(8,128)(2,1)S(1)} %slice.520), channel_id=1, source_target_pairs={{0,8},{8,16},{16,24},{24,32},{32,40},{40,48},{48,56},{56,64},{64,7... | collective-permute-start | bytes 34568 | tf_op jit(solution)/shard_map/ppermute | solution.py:16
  5.2 4.5 %collective-permute-done = bf16[30,192]{0,1:T(8,128)(2,1)S(1)} collective-permute-done((bf16[30,192]{0,1:T(8,128)(2,1)S(1)}, bf16[30,192]{0,1:T(8,128)(2,1)S(1)}, u32[]{:S(2)}, u32[]{:S(2)}) %collective-permute-start) | collective-permute-done | bytes 11552 | tf_op jit(solution)/shard_map/ppermute | solution.py:16
  9.8 1.8 %add_convert_fusion = bf16[128,192]{0,1:T(8,128)(2,1)S(1)} fusion(f32[158,192]{0,1:T(8,128)S(1)} %maximum_convert_fusion, f32[192]{0:T(256)S(1)} %bitcast.161, f32[192]{0:T(256)S(1)} %bitcast.163, f32[192]{0:T(256)S(1)} %bitcast.105, f32[192]{0:T(256)S(1)} %bitcast.107, f32[192]{0:T(256)S(1)} %bitcast.109, f32[192]{0:T(256)S(1)} %bitcast.111, ...), kind=kLoop, calls=%fused_computation.168 | loop fusion | flops 1523712 | bytes 3120384 | tf_op jit(solution)/shard_map/convert_element_type | solution.py:72
  11.7 0.6 broadcast_in_dim.24
  12.3 4.3 %all-to-all-start = ((f32[8,1,256]{2,1,0:T(1,128)}), f32[8,1,256]{2,1,0:T(1,128)S(1)}, u32[]{:S(2)}, u32[]{:S(2)}) async-start(f32[8,1,256]{2,1,0:T(1,128)} %broadcast_in_dim.24), calls=%async_computation | async-start | bytes 16384 | tf_op jit(solution)/shard_map/all_to_all | solution.py:20
  16.7 5.2 %all-to-all-done = f32[8,1,256]{2,1,0:T(1,128)S(1)} async-done(((f32[8,1,256]{2,1,0:T(1,128)}), f32[8,1,256]{2,1,0:T(1,128)S(1)}, u32[]{:S(2)}, u32[]{:S(2)}) %all-to-all-start) | async-done | bytes 8224 | tf_op jit(solution)/shard_map/all_to_all | solution.py:20
  21.9 0.8 broadcast_in_dim.25
  22.7 16.0 %all-to-all-start.1 = ((bf16[16,96,128]{2,1,0:T(8,128)(2,1)}), bf16[16,96,128]{2,1,0:T(8,128)(2,1)S(1)}, u32[]{:S(2)}, u32[]{:S(2)}) async-start(bf16[16,96,128]{2,1,0:T(8,128)(2,1)} %broadcast_in_dim.25), calls=%async_computation.1 | async-start | bytes 786432 | tf_op jit(solution)/shard_map/all_to_all | solution.py:20
  38.7 0.7 copy.27
  39.4 1.3 copy.29
  40.8 20.6 %all-to-all-done.1 = bf16[16,96,128]{2,1,0:T(8,128)(2,1)S(1)} async-done(((bf16[16,96,128]{2,1,0:T(8,128)(2,1)}), bf16[16,96,128]{2,1,0:T(8,128)(2,1)S(1)}, u32[]{:S(2)}, u32[]{:S(2)}) %all-to-all-start.1) | async-done | bytes 393248 | tf_op jit(solution)/shard_map/all_to_all | solution.py:20
  61.4 3.5 %all-to-all-start.2 = ((bf16[4,128,1024]{2,1,0:T(8,128)(2,1)}), bf16[4,128,1024]{2,1,0:T(8,128)(2,1)S(1)}, u32[]{:S(2)}, u32[]{:S(2)}) async-start(bf16[4,128,1024]{2,1,0:T(8,128)(2,1)} %copy.29), calls=%async_computation.2 | async-start | bytes 2097152 | tf_op jit(solution)/shard_map/all_to_all | solution.py:20
  65.0 0.1 fusion.92
  65.1 0.1 maximum_maximum_fusion
  65.2 10.6 %all-to-all-done.2 = bf16[4,128,1024]{2,1,0:T(8,128)(2,1)S(1)} async-done(((bf16[4,128,1024]{2,1,0:T(8,128)(2,1)}), bf16[4,128,1024]{2,1,0:T(8,128)(2,1)S(1)}, u32[]{:S(2)}, u32[]{:S(2)}) %all-to-all-start.2) | async-done | bytes 1048608 | tf_op jit(solution)/shard_map/all_to_all | solution.py:20
  75.8 0.5 fusion.2
  76.3 0.7 copy.41
  77.0 3.4 %all-to-all-start.3 = ((bf16[4,128,192]{1,2,0:T(8,128)(2,1)}), bf16[4,128,192]{1,2,0:T(8,128)(2,1)S(1)}, u32[]{:S(2)}, u32[]{:S(2)}) async-start(bf16[4,128,192]{1,2,0:T(8,128)(2,1)} %bitcast.90), calls=%async_computation.3 | async-start | bytes 393216 | tf_op jit(solution)/shard_map/all_to_all | solution.py:20
  80.4 6.3 %all-to-all-done.3 = bf16[4,128,192]{1,2,0:T(8,128)(2,1)S(1)} async-done(((bf16[4,128,192]{1,2,0:T(8,128)(2,1)}), bf16[4,128,192]{1,2,0:T(8,128)(2,1)S(1)}, u32[]{:S(2)}, u32[]{:S(2)}) %all-to-all-start.3) | async-done | bytes 196640 | tf_op jit(solution)/shard_map/all_to_all | solution.py:20
  86.7 0.7 copy-done.5
  87.4 0.2 fusion.27
  87.6 7.7 %all_to_all.52 = f32[8,1,256]{2,1,0:T(1,128)S(1)} all-to-all(f32[8,1,256]{2,1,0:T(1,128)S(1)} %broadcast_in_dim.26), channel_id=1, replica_groups=mesh['sp_0'=16,'sp_1'=4,'dp'=8] {'dp'}, dimensions={0} | all-to-all | bytes 16384 | tf_op jit(solution)/shard_map/all_to_all | solution.py:20
  95.4 0.9 fusion.57
  96.3 1.2 fusion.58
  97.5 0.1 stack.131
  97.6 7.8 %all_to_all.53 = f32[4,8,192]{2,1,0:T(8,128)S(1)} all-to-all(f32[4,8,192]{2,1,0:T(8,128)S(1)} %bitcast.102), channel_id=1, replica_groups=mesh['sp_0'=16,'sp_1'=4,'dp'=8] {'sp_1'}, dimensions={0} | all-to-all | bytes 49152 | tf_op jit(solution)/shard_map/all_to_all | solution.py:20
  105.4 0.7 broadcast_in_dim.27
  106.1 3.4 %all-to-all-start.5 = ((bf16[4,128,192]{1,2,0:T(8,128)(2,1)}), bf16[4,128,192]{1,2,0:T(8,128)(2,1)S(1)}, u32[]{:S(2)}, u32[]{:S(2)}) async-start(bf16[4,128,192]{1,2,0:T(8,128)(2,1)} %broadcast_in_dim.27), calls=%async_computation.5 | async-start | bytes 393216 | tf_op jit(solution)/shard_map/all_to_all | solution.py:20
  109.5 6.3 %all-to-all-done.5 = bf16[4,128,192]{1,2,0:T(8,128)(2,1)S(1)} async-done(((bf16[4,128,192]{1,2,0:T(8,128)(2,1)}), bf16[4,128,192]{1,2,0:T(8,128)(2,1)S(1)}, u32[]{:S(2)}, u32[]{:S(2)}) %all-to-all-start.5) | async-done | bytes 196640 | tf_op jit(solution)/shard_map/all_to_all | solution.py:20
  115.8 0.6 broadcast_in_dim.28
  116.4 11.3 %all-to-all-start.8 = ((bf16[16,8,192]{2,1,0:T(8,128)(2,1)}), bf16[16,8,192]{2,1,0:T(8,128)(2,1)S(1)}, u32[]{:S(2)}, u32[]{:S(2)}) async-start(bf16[16,8,192]{2,1,0:T(8,128)(2,1)} %broadcast_in_dim.28), calls=%async_computation.8 | async-start | bytes 131072 | tf_op jit(solution)/shard_map/all_to_all | solution.py:20
  127.7 0.4 fusion.1
  128.1 0.2 copy.32
  128.5 10.4 %all-to-all-done.8 = bf16[16,8,192]{2,1,0:T(8,128)(2,1)S(1)} async-done(((bf16[16,8,192]{2,1,0:T(8,128)(2,1)}), bf16[16,8,192]{2,1,0:T(8,128)(2,1)S(1)}, u32[]{:S(2)}, u32[]{:S(2)}) %all-to-all-start.8) | async-done | bytes 49184 | tf_op jit(solution)/shard_map/all_to_all | solution.py:20
  138.9 0.6 broadcast_in_dim.29
  139.5 3.3 %all-to-all-start.9 = ((f32[4,8,192]{2,1,0:T(8,128)}), f32[4,8,192]{2,1,0:T(8,128)S(1)}, u32[]{:S(2)}, u32[]{:S(2)}) async-start(f32[4,8,192]{2,1,0:T(8,128)} %broadcast_in_dim.29), calls=%async_computation.9 | async-start | bytes 65536 | tf_op jit(solution)/shard_map/all_to_all | solution.py:20
  142.8 0.8 maximum_maximum_fusion.1
  143.6 4.6 %all-to-all-done.9 = f32[4,8,192]{2,1,0:T(8,128)S(1)} async-done(((f32[4,8,192]{2,1,0:T(8,128)}), f32[4,8,192]{2,1,0:T(8,128)S(1)}, u32[]{:S(2)}, u32[]{:S(2)}) %all-to-all-start.9) | async-done | bytes 24608 | tf_op jit(solution)/shard_map/all_to_all | solution.py:20
  148.2 5.2 %all-to-all-start.6 = ((bf16[16,96,128]{2,1,0:T(8,128)(2,1)}), bf16[16,96,128]{2,1,0:T(8,128)(2,1)S(1)}, u32[]{:S(2)}, u32[]{:S(2)}) async-start(bf16[16,96,128]{2,1,0:T(8,128)(2,1)} %maximum_maximum_fusion.1), calls=%async_computation.6 | async-start | bytes 786432 | tf_op jit(solution)/shard_map/all_to_all | solution.py:20
  153.4 3.1 %collective-permute-start.1 = (bf16[30,192]{0,1:T(8,128)(2,1)S(1)}, bf16[30,192]{0,1:T(8,128)(2,1)S(1)}, u32[]{:S(2)}, u32[]{:S(2)}) collective-permute-start(bf16[30,192]{0,1:T(8,128)(2,1)S(1)} %bitcast.99), channel_id=1, source_target_pairs={{8,0},{16,8},{24,16},{32,24},{40,32},{48,40},{56,48},{64,56},{72,6... | collective-permute-start | bytes 34568 | tf_op jit(solution)/shard_map/ppermute | solution.py:16
  156.5 8.7 %collective-permute-done.1 = bf16[30,192]{0,1:T(8,128)(2,1)S(1)} collective-permute-done((bf16[30,192]{0,1:T(8,128)(2,1)S(1)}, bf16[30,192]{0,1:T(8,128)(2,1)S(1)}, u32[]{:S(2)}, u32[]{:S(2)}) %collective-permute-start.1) | collective-permute-done | bytes 11552 | tf_op jit(solution)/shard_map/ppermute | solution.py:16
  165.2 1.8 %fusion.60 = bf16[128,192]{0,1:T(8,128)(2,1)S(1)} fusion(f32[158,192]{0,1:T(8,128)S(1)} %maximum_convert_fusion.1, f32[192]{0:T(256)S(1)} %bitcast.162, f32[192]{0:T(256)S(1)} %bitcast.164, f32[192]{0:T(256)S(1)} %bitcast.106, f32[192]{0:T(256)S(1)} %bitcast.108, f32[192]{0:T(256)S(1)} %bitcast.110, f32[192]{0:T(256)S(1)} %bitcast.112, ...), kind=kLoop, calls=%fused_computation.106 | loop fusion | flops 1523712 | bytes 3120384 | tf_op jit(solution)/shard_map/convert_element_type | solution.py:119
  167.1 0.7 fusion.7
  167.8 0.6 slice.594
  168.3 4.8 %all-to-all-done.6 = bf16[16,96,128]{2,1,0:T(8,128)(2,1)S(1)} async-done(((bf16[16,96,128]{2,1,0:T(8,128)(2,1)}), bf16[16,96,128]{2,1,0:T(8,128)(2,1)S(1)}, u32[]{:S(2)}, u32[]{:S(2)}) %all-to-all-start.6) | async-done | bytes 393248 | tf_op jit(solution)/shard_map/all_to_all | solution.py:20
  173.3 0.6 maximum_maximum_fusion.2
  174.0 0.6 copy.43
  (39 shorter events, 1.0 us)
Async XLA Ops:
  1.5 3.6 %copy-start.3 = (bf16[64,192]{1,0:T(8,128)(2,1)S(1)}, bf16[64,192]{1,0:T(8,128)(2,1)}, u32[]{:S(2)}) copy-start(bf16[64,192]{1,0:T(8,128)(2,1)} %param.9) | copy-start | bytes 73732
  1.6 3.5 %copy-start.4 = (f32[31,192]{1,0:T(8,128)S(1)}, f32[31,192]{1,0:T(8,128)}, u32[]{:S(2)}) copy-start(f32[31,192]{1,0:T(8,128)} %param.10) | copy-start | bytes 71428
  1.6 8.1 %collective-permute-start = (bf16[30,192]{0,1:T(8,128)(2,1)S(1)}, bf16[30,192]{0,1:T(8,128)(2,1)S(1)}, u32[]{:S(2)}, u32[]{:S(2)}) collective-permute-start(bf16[30,192]{0,1:T(8,128)(2,1)S(1)} %slice.520), channel_id=1, source_target_pairs={{0,8},{8,16},{16,24},{24,32},{32,40},{40,48},{48,56},{56,64},{64,7... | collective-permute-start | bytes 34568 | tf_op jit(solution)/shard_map/ppermute | solution.py:16
  9.8 6.8 %slice-start = ((bf16[64,192]{1,0:T(8,128)(2,1)}), bf16[64,128]{1,0:T(8,128)(2,1)S(1)}, s32[]{:S(2)}) async-start(bf16[64,192]{1,0:T(8,128)(2,1)} %param.9), calls=%async_computation.10 | async-start | bytes 32768 | tf_op jit(solution)/shard_map/slice | solution.py:40
  11.6 27.1 %copy-start = (bf16[128,4096]{1,0:T(8,128)(2,1)S(1)}, bf16[128,4096]{1,0:T(8,128)(2,1)}, u32[]{:S(2)}) copy-start(bf16[128,4096]{1,0:T(8,128)(2,1)} %param.8) | copy-start | bytes 3145732
  12.3 9.6 %all-to-all-start = ((f32[8,1,256]{2,1,0:T(1,128)}), f32[8,1,256]{2,1,0:T(1,128)S(1)}, u32[]{:S(2)}, u32[]{:S(2)}) async-start(f32[8,1,256]{2,1,0:T(1,128)} %broadcast_in_dim.24), calls=%async_computation | async-start | bytes 16384 | tf_op jit(solution)/shard_map/all_to_all | solution.py:20
  22.7 38.7 %all-to-all-start.1 = ((bf16[16,96,128]{2,1,0:T(8,128)(2,1)}), bf16[16,96,128]{2,1,0:T(8,128)(2,1)S(1)}, u32[]{:S(2)}, u32[]{:S(2)}) async-start(bf16[16,96,128]{2,1,0:T(8,128)(2,1)} %broadcast_in_dim.25), calls=%async_computation.1 | async-start | bytes 786432 | tf_op jit(solution)/shard_map/all_to_all | solution.py:20
  61.4 14.4 %all-to-all-start.2 = ((bf16[4,128,1024]{2,1,0:T(8,128)(2,1)}), bf16[4,128,1024]{2,1,0:T(8,128)(2,1)S(1)}, u32[]{:S(2)}, u32[]{:S(2)}) async-start(bf16[4,128,1024]{2,1,0:T(8,128)(2,1)} %copy.29), calls=%async_computation.2 | async-start | bytes 2097152 | tf_op jit(solution)/shard_map/all_to_all | solution.py:20
  77.0 9.7 %all-to-all-start.3 = ((bf16[4,128,192]{1,2,0:T(8,128)(2,1)}), bf16[4,128,192]{1,2,0:T(8,128)(2,1)S(1)}, u32[]{:S(2)}, u32[]{:S(2)}) async-start(bf16[4,128,192]{1,2,0:T(8,128)(2,1)} %bitcast.90), calls=%async_computation.3 | async-start | bytes 393216 | tf_op jit(solution)/shard_map/all_to_all | solution.py:20
  86.7 0.7 copy-start.5
  106.1 9.7 %all-to-all-start.5 = ((bf16[4,128,192]{1,2,0:T(8,128)(2,1)}), bf16[4,128,192]{1,2,0:T(8,128)(2,1)S(1)}, u32[]{:S(2)}, u32[]{:S(2)}) async-start(bf16[4,128,192]{1,2,0:T(8,128)(2,1)} %broadcast_in_dim.27), calls=%async_computation.5 | async-start | bytes 393216 | tf_op jit(solution)/shard_map/all_to_all | solution.py:20
  116.4 22.4 %all-to-all-start.8 = ((bf16[16,8,192]{2,1,0:T(8,128)(2,1)}), bf16[16,8,192]{2,1,0:T(8,128)(2,1)S(1)}, u32[]{:S(2)}, u32[]{:S(2)}) async-start(bf16[16,8,192]{2,1,0:T(8,128)(2,1)} %broadcast_in_dim.28), calls=%async_computation.8 | async-start | bytes 131072 | tf_op jit(solution)/shard_map/all_to_all | solution.py:20
  139.5 8.7 %all-to-all-start.9 = ((f32[4,8,192]{2,1,0:T(8,128)}), f32[4,8,192]{2,1,0:T(8,128)S(1)}, u32[]{:S(2)}, u32[]{:S(2)}) async-start(f32[4,8,192]{2,1,0:T(8,128)} %broadcast_in_dim.29), calls=%async_computation.9 | async-start | bytes 65536 | tf_op jit(solution)/shard_map/all_to_all | solution.py:20
  148.2 25.0 %all-to-all-start.6 = ((bf16[16,96,128]{2,1,0:T(8,128)(2,1)}), bf16[16,96,128]{2,1,0:T(8,128)(2,1)S(1)}, u32[]{:S(2)}, u32[]{:S(2)}) async-start(bf16[16,96,128]{2,1,0:T(8,128)(2,1)} %maximum_maximum_fusion.1), calls=%async_computation.6 | async-start | bytes 786432 | tf_op jit(solution)/shard_map/all_to_all | solution.py:20
  153.4 11.8 %collective-permute-start.1 = (bf16[30,192]{0,1:T(8,128)(2,1)S(1)}, bf16[30,192]{0,1:T(8,128)(2,1)S(1)}, u32[]{:S(2)}, u32[]{:S(2)}) collective-permute-start(bf16[30,192]{0,1:T(8,128)(2,1)S(1)} %bitcast.99), channel_id=1, source_target_pairs={{8,0},{16,8},{24,16},{32,24},{40,32},{48,40},{56,48},{64,56},{72,6... | collective-permute-start | bytes 34568 | tf_op jit(solution)/shard_map/ppermute | solution.py:16
  165.2 1.8 %copy-start.1 = (bf16[128,192]{0,1:T(8,128)(2,1)S(1)}, bf16[128,192]{0,1:T(8,128)(2,1)}, u32[]{:S(2)}) copy-start(bf16[128,192]{0,1:T(8,128)(2,1)} %param.6) | copy-start | bytes 147460
  165.2 1.8 %copy-start.2 = (bf16[128,192]{0,1:T(8,128)(2,1)S(1)}, bf16[128,192]{0,1:T(8,128)(2,1)}, u32[]{:S(2)}) copy-start(bf16[128,192]{0,1:T(8,128)(2,1)} %param.7) | copy-start | bytes 147460

commit v2 on v1

--- a/solution.py
+++ b/solution.py
@@ -3,6 +3,7 @@
 from jax import lax
 from jax.sharding import Mesh
 from jax.sharding import PartitionSpec as P
+
 
 SP = ("sp_0", "sp_1")
 
@@ -24,14 +25,16 @@
     return exchange(jnp.broadcast_to(array, (lax.axis_size(axis), *array.shape)), axis)
 
 
-def packed_total(arrays, axis):
-    ravelled = jnp.concatenate([a.reshape(-1) for a in arrays])
-    total = from_everyone(ravelled, axis).sum(axis=0)
-    at, finished = 0, []
-    for a in arrays:
-        finished.append(total[at : at + a.size].reshape(a.shape))
-        at += a.size
-    return tuple(finished)
+def shifted(value, axis, steps):
+    count = lax.axis_size(axis)
+    return lax.ppermute(value, axis, [(i, (i + steps) % count) for i in range(count)])
+
+
+def chip_pairs_total(value, axis):
+    count = lax.axis_size(axis)
+    value = value + lax.ppermute(value, axis, [(i, i ^ 1) for i in range(count)])
+    others = [shifted(value, axis, k) for k in range(2, count, 2)]
+    return sum(others, value)
 
 
 def dense(blocks):
@@ -55,10 +58,14 @@
     z_size, y_size = (lax.axis_size("sp_0"), lax.axis_size("sp_1"))
     d_rows = out_weight.shape[0]
 
-    weight = undense(from_everyone(dense(out_weight), "sp_0")).reshape(z_size * d_rows, width_dp)
-    columns = cotangent.reshape(rows_here, z_size, y_size, d_rows).transpose(2, 0, 1, 3)
-    columns = exchange(columns.reshape(y_size, rows_here, z_size * d_rows), "sp_1")
-    columns = columns.reshape(y_size * rows_here, z_size * d_rows)
+    y_here = lax.axis_index("sp_1")
+    ahead = range(1, y_size)
+
+    weight = from_everyone(dense(out_weight), "sp_0")
+    blocks = cotangent.reshape(rows_here, z_size, y_size, d_rows).transpose(2, 0, 1, 3)
+    blocks = blocks.reshape(y_size, rows_here, z_size * d_rows)
+    blocks = [lax.dynamic_index_in_dim(blocks, (y_here + k) % y_size, 0, False) for k in range(y_size)]
+    columns = [blocks[0]] + [shifted(blocks[k], "sp_1", k) for k in ahead]
 
     sigma_gate = jax.nn.sigmoid(gate_input.astype(jnp.float32))
     mixed_in = (val_input.astype(jnp.float32) * sigma_gate).astype(jnp.bfloat16)
@@ -70,7 +77,8 @@
     for offset in range(taps):
         conv_out = conv_out + conv_taps[offset][None, :] * padded_in[offset : offset + rows_here]
     conv_rows = lax.optimization_barrier(conv_out.astype(jnp.bfloat16)).astype(jnp.float32)
-    row_sums = packed_total((jnp.sum(conv_rows, 1), jnp.sum(conv_rows * conv_rows, 1)), "dp")
+    row_sums = jnp.stack([jnp.sum(conv_rows, 1), jnp.sum(conv_rows * conv_rows, 1)])
+    row_sums = chip_pairs_total(row_sums, "dp")
     row_mean = row_sums[0][:, None] / channels
     row_var = row_sums[1][:, None] / channels - row_mean * row_mean
     inv_scale = lax.rsqrt(row_var + norm_floor)
@@ -79,38 +87,51 @@
     sigma_act = jax.nn.sigmoid(act)
     swished = (act * sigma_act).astype(jnp.bfloat16)
 
-    swished_y = from_everyone(swished, "sp_1").reshape(y_size * rows_here, width_dp)
+    swished_y = jnp.concatenate([swished] + [shifted(swished, "sp_1", k) for k in ahead], 0)
     weight_part = lax.dot_general(
-        columns, swished_y, (((0,), (0,)), ((), ())), preferred_element_type=jnp.float32
+        jnp.concatenate(columns, 0),
+        swished_y,
+        (((0,), (0,)), ((), ())),
+        preferred_element_type=jnp.float32,
     )
     weight_part = weight_part.astype(jnp.bfloat16).reshape(z_size, d_rows, width_dp)
-    weight_part = exchange(dense(weight_part), "sp_0").astype(jnp.float32)
-    grad_out_weight = undense(weight_part.sum(axis=0))
+    weight, weight_part = lax.optimization_barrier((weight, dense(weight_part)))
+    weight = undense(weight).reshape(z_size * d_rows, width_dp)
+    weight_part = exchange(weight_part, "sp_0")
 
-    mix_part = jnp.dot(columns, weight, preferred_element_type=jnp.float32).astype(jnp.bfloat16)
-    mix_part = exchange(mix_part.reshape(y_size, rows_here, width_dp), "sp_1")
-    grad_mix = mix_part.astype(jnp.float32).sum(axis=0)
+    mix_parts = [
+        jnp.dot(c, weight, preferred_element_type=jnp.float32).astype(jnp.bfloat16) for c in columns
+    ]
+    mix_parts = [mix_parts[0]] + [shifted(mix_parts[k], "sp_1", -k) for k in ahead]
+    grad_mix = sum(p.astype(jnp.float32) for p in mix_parts)
 
     grad_act = grad_mix * sigma_act * (1.0 + act * (1.0 - sigma_act))
     gain_part = jnp.sum(grad_act * normed, 0)
     grad_norm = grad_act * norm_gain[None, :]
-    norm_sums = packed_total((jnp.sum(grad_norm, 1), jnp.sum(grad_norm * normed, 1)), "dp")
+    norm_sums = jnp.stack([jnp.sum(grad_norm, 1), jnp.sum(grad_norm * normed, 1)])
+    norm_sums = chip_pairs_total(norm_sums, "dp")
     first_sum = norm_sums[0][:, None] / channels
     second_sum = norm_sums[1][:, None] / channels
     grad_conv = (inv_scale * (grad_norm - first_sum - normed * second_sum)).astype(jnp.bfloat16)
     grad_conv = lax.optimization_barrier(grad_conv)
+    later = passed_along(grad_conv[: taps - 1], SP, -1)
     own_grad = grad_conv.astype(jnp.float32)
     tap_list = []
     for offset in range(taps):
         tap_list.append(jnp.sum(own_grad * padded_in[offset : offset + rows_here], 0))
     tail = jnp.stack(tap_list + [gain_part], 0)
     tail = tail.reshape(y_size, (taps + 1) // y_size, width_dp)
-    tail = exchange(tail, "sp_1").sum(axis=0).astype(jnp.bfloat16)
+    tail = [lax.dynamic_index_in_dim(tail, (y_here + k) % y_size, 0, False) for k in range(y_size)]
+    tail = sum([shifted(tail[k], "sp_1", k) for k in ahead], tail[0]).astype(jnp.bfloat16)
+    tail, weight_part = lax.optimization_barrier((tail, weight_part))
+    grad_out_weight = undense(weight_part.astype(jnp.float32).sum(axis=0))
     tail = from_everyone(tail, "sp_0").astype(jnp.float32).sum(axis=0)
-    tail = from_everyone(tail, "sp_1").reshape(taps + 1, width_dp)
+    tail = jnp.stack([tail] + [shifted(tail, "sp_1", -k) for k in ahead])
+    tail = jnp.concatenate([tail, tail], 0)
+    tail = lax.dynamic_slice_in_dim(tail, (y_size - y_here) % y_size, y_size, 0)
+    tail = tail.reshape(taps + 1, width_dp)
     grad_taps, grad_gain = (tail[:taps], tail[taps])
 
-    later = passed_along(grad_conv[: taps - 1], SP, -1)
     padded_grad = jnp.concatenate([grad_conv, later], 0).astype(jnp.float32)
     grad_mixed = jnp.zeros((rows_here, width_dp), jnp.float32)
     for offset in range(taps):
@@ -128,6 +149,7 @@
     split = Mesh(mesh.devices.reshape(16, 4, mesh.shape["dp"]), ("sp_0", "sp_1", "dp"))
     in_specs = (P(SP, "dp"), P(SP, "dp"), P(SP, None), P(SP, "dp"), P(None, "dp"), P("dp"))
     out_specs = (P(SP, "dp"), P(SP, "dp"), P(SP, "dp"), P(None, "dp"), P("dp"))
+
     return jax.shard_map(
         per_device, mesh=split, in_specs=in_specs, out_specs=out_specs, check_vma=False
     )

time: 176 us -> 173 us (0.983)
  the two profiles are of different devices: /device:TPU:64 before, /device:TPU:4 now
where the time goes in v2:
time: 173 us; the launch traced here: 172 us
  starting transfers between devices  114 us (66%)
  waiting for transfers between devices  41.3 us (24%)
  other arithmetic  8.88 us (5%)
  local copies, waits for them, and re-layouts  4.61 us (3%)
  matrix products  1.82 us (1%)
    ppermute x21, starting transfers between devices, shifted(): lax.ppermute(value, axis, [(i, (i + steps) % count) for i in range(count)])  71.3 us
    all_to_all x3, starting transfers between devices, exchange(): return lax.all_to_all(blocks, axis, split_axis=0, concat_axis=0, tiled=True)  36.3 us
    all_to_all x3, waiting for transfers between devices, exchange(): return lax.all_to_all(blocks, axis, split_axis=0, concat_axis=0, tiled=True)  16.3 us
    ppermute x21, waiting for transfers between devices, shifted(): lax.ppermute(value, axis, [(i, (i + steps) % count) for i in range(count)])  12.4 us
    ppermute x2, waiting for transfers between devices, passed_along(): lax.ppermute(value, axis, [(source, source + steps) for source in range(f...  10.3 us
    ppermute x2, starting transfers between devices, chip_pairs_total(): lax.ppermute(value, axis, [(i, i ^ 1) for i in range(count)])  3.84 us
  transfers between devices with their start and end apart: 28, of which 13 were waited for; matrix products, arithmetic and copies ran while one was open for 7% of the time, Pallas kernels for 0%

profile of v2, /device:TPU:4, one launch (start us, length us, event | category | flops | bytes accessed | tf_op | source)
XLA Modules:
  0.0 172.4 jit_solution(12569892980739267670)
XLA Ops:
  0.7 1.6 copy.14
  2.5 3.5 %collective-permute-start.5 = (bf16[128,1024]{0,1:T(8,128)(2,1)S(1)}, bf16[128,1024]{0,1:T(8,128)(2,1)S(1)}, u32[]{:S(2)}, u32[]{:S(2)}) collective-permute-start(bf16[128,1024]{0,1:T(8,128)(2,1)S(1)} %get-tuple-element.53), channel_id=1, source_target_pairs={{0,8},{8,16},{16,24},{24,0},{1,9},{9,17},{17,25},{25,1},{2,10},{10... | collective-permute-start | bytes 786440 | tf_op jit(solution)/shard_map/ppermute | solution.py:30
  6.0 4.8 %collective-permute-start.6 = (bf16[128,1024]{0,1:T(8,128)(2,1)S(1)}, bf16[128,1024]{0,1:T(8,128)(2,1)S(1)}, u32[]{:S(2)}, u32[]{:S(2)}) collective-permute-start(bf16[128,1024]{0,1:T(8,128)(2,1)S(1)} %get-tuple-element.52), channel_id=1, source_target_pairs={{0,16},{8,24},{16,0},{24,8},{1,17},{9,25},{17,1},{25,9},{2,18},{10... | collective-permute-start | bytes 786440 | tf_op jit(solution)/shard_map/ppermute | solution.py:30
  11.0 1.5 collective-permute-start
  12.6 5.7 %collective-permute-done = bf16[30,192]{0,1:T(8,128)(2,1)S(1)} collective-permute-done((bf16[30,192]{0,1:T(8,128)(2,1)S(1)}, bf16[30,192]{0,1:T(8,128)(2,1)S(1)}, u32[]{:S(2)}, u32[]{:S(2)}) %collective-permute-start) | collective-permute-done | bytes 11552 | tf_op jit(solution)/shard_map/ppermute | solution.py:17
  18.4 1.8 %add_convert_fusion = bf16[128,192]{0,1:T(8,128)(2,1)S(1)} fusion(f32[158,192]{0,1:T(8,128)S(1)} %maximum_convert_fusion, f32[192]{0:T(256)S(1)} %bitcast.205, f32[192]{0:T(256)S(1)} %bitcast.207, f32[192]{0:T(256)S(1)} %bitcast.149, f32[192]{0:T(256)S(1)} %bitcast.151, f32[192]{0:T(256)S(1)} %bitcast.153, f32[192]{0:T(256)S(1)} %bitcast.155, ...), kind=kLoop, calls=%fused_computation.185 | loop fusion | flops 1523712 | bytes 3120384 | tf_op jit(solution)/shard_map/convert_element_type | solution.py:79
  20.3 1.9 %collective-permute-start.1 = (f32[2,128]{1,0:T(2,128)S(1)}, f32[2,128]{1,0:T(2,128)S(1)}, u32[]{:S(2)}, u32[]{:S(2)}) collective-permute-start(f32[2,128]{1,0:T(2,128)S(1)} %pad_maximum_fusion), channel_id=1, source_target_pairs={{0,1},{1,0},{2,3},{3,2},{4,5},{5,4},{6,7},{7,6},{8,9},{9,8},{10,11... | collective-permute-start | bytes 3080 | tf_op jit(solution)/shard_map/ppermute | solution.py:35
  22.2 1.1 collective-permute-done.1
  23.4 3.1 %collective-permute-start.2 = (f32[2,128]{1,0:T(2,128)S(1)}, f32[2,128]{1,0:T(2,128)S(1)}, u32[]{:S(2)}, u32[]{:S(2)}) collective-permute-start(f32[2,128]{1,0:T(2,128)S(1)} %fusion.109), channel_id=1, source_target_pairs={{0,2},{1,3},{2,4},{3,5},{4,6},{5,7},{6,0},{7,1},{8,10},{9,11},{10,... | collective-permute-start | bytes 3080 | tf_op jit(solution)/shard_map/ppermute | solution.py:30
  26.5 3.0 %collective-permute-start.3 = (f32[2,128]{1,0:T(2,128)S(1)}, f32[2,128]{1,0:T(2,128)S(1)}, u32[]{:S(2)}, u32[]{:S(2)}) collective-permute-start(f32[2,128]{1,0:T(2,128)S(1)} %fusion.109), channel_id=1, source_target_pairs={{0,4},{1,5},{2,6},{3,7},{4,0},{5,1},{6,2},{7,3},{8,12},{9,13},{10,... | collective-permute-start | bytes 3080 | tf_op jit(solution)/shard_map/ppermute | solution.py:30
  29.4 4.5 %collective-permute-start.4 = (f32[2,128]{1,0:T(2,128)S(1)}, f32[2,128]{1,0:T(2,128)S(1)}, u32[]{:S(2)}, u32[]{:S(2)}) collective-permute-start(f32[2,128]{1,0:T(2,128)S(1)} %fusion.109), channel_id=1, source_target_pairs={{0,6},{1,7},{2,0},{3,1},{4,2},{5,3},{6,4},{7,5},{8,14},{9,15},{10,... | collective-permute-start | bytes 3080 | tf_op jit(solution)/shard_map/ppermute | solution.py:30
  34.1 0.8 broadcast_in_dim.8
  34.8 15.9 %all-to-all-start = ((bf16[16,96,128]{2,1,0:T(8,128)(2,1)}), bf16[16,96,128]{2,1,0:T(8,128)(2,1)S(1)}, u32[]{:S(2)}, u32[]{:S(2)}) async-start(bf16[16,96,128]{2,1,0:T(8,128)(2,1)} %broadcast_in_dim.8), calls=%async_computation | async-start | bytes 786432 | tf_op jit(solution)/shard_map/all_to_all | solution.py:21
  50.8 3.7 %collective-permute-start.7 = (bf16[128,1024]{0,1:T(8,128)(2,1)S(1)}, bf16[128,1024]{0,1:T(8,128)(2,1)S(1)}, u32[]{:S(2)}, u32[]{:S(2)}) collective-permute-start(bf16[128,1024]{0,1:T(8,128)(2,1)S(1)} %get-tuple-element.51), channel_id=1, source_target_pairs={{0,24},{8,0},{16,8},{24,16},{1,25},{9,1},{17,9},{25,17},{2,26},{10... | collective-permute-start | bytes 786440 | tf_op jit(solution)/shard_map/ppermute | solution.py:30
  54.7 2.3 %collective-permute-start.10 = (bf16[128,192]{0,1:T(8,128)(2,1)S(1)}, bf16[128,192]{0,1:T(8,128)(2,1)S(1)}, u32[]{:S(2)}, u32[]{:S(2)}) collective-permute-start(bf16[128,192]{0,1:T(8,128)(2,1)S(1)} %fusion.32), channel_id=1, source_target_pairs={{0,24},{8,0},{16,8},{24,16},{1,25},{9,1},{17,9},{25,17},{2,26},{10... | collective-permute-start | bytes 147464 | tf_op jit(solution)/shard_map/ppermute | solution.py:30
  57.0 3.6 %collective-permute-start.8 = (bf16[128,192]{0,1:T(8,128)(2,1)S(1)}, bf16[128,192]{0,1:T(8,128)(2,1)S(1)}, u32[]{:S(2)}, u32[]{:S(2)}) collective-permute-start(bf16[128,192]{0,1:T(8,128)(2,1)S(1)} %fusion.32), channel_id=1, source_target_pairs={{0,8},{8,16},{16,24},{24,0},{1,9},{9,17},{17,25},{25,1},{2,10},{10... | collective-permute-start | bytes 147464 | tf_op jit(solution)/shard_map/ppermute | solution.py:30
  61.0 3.5 %collective-permute-start.9 = (bf16[128,192]{0,1:T(8,128)(2,1)S(1)}, bf16[128,192]{0,1:T(8,128)(2,1)S(1)}, u32[]{:S(2)}, u32[]{:S(2)}) collective-permute-start(bf16[128,192]{0,1:T(8,128)(2,1)S(1)} %fusion.32), channel_id=1, source_target_pairs={{0,16},{8,24},{16,0},{24,8},{1,17},{9,25},{17,1},{25,9},{2,18},{10... | collective-permute-start | bytes 147464 | tf_op jit(solution)/shard_map/ppermute | solution.py:30
  64.5 4.0 %collective-permute-done.9 = bf16[128,192]{0,1:T(8,128)(2,1)S(1)} collective-permute-done((bf16[128,192]{0,1:T(8,128)(2,1)S(1)}, bf16[128,192]{0,1:T(8,128)(2,1)S(1)}, u32[]{:S(2)}, u32[]{:S(2)}) %collective-permute-start.9) | collective-permute-done | bytes 49184 | tf_op jit(solution)/shard_map/ppermute | solution.py:30
  69.3 0.9 maximum_maximum_fusion.1
  70.2 3.3 %all-to-all-done = bf16[16,96,128]{2,1,0:T(8,128)(2,1)S(1)} async-done(((bf16[16,96,128]{2,1,0:T(8,128)(2,1)}), bf16[16,96,128]{2,1,0:T(8,128)(2,1)S(1)}, u32[]{:S(2)}, u32[]{:S(2)}) %all-to-all-start) | async-done | bytes 393248 | tf_op jit(solution)/shard_map/all_to_all | solution.py:21
  74.0 3.7 %collective-permute-start.11 = (bf16[128,192]{0,1:T(8,128)(2,1)S(1)}, bf16[128,192]{0,1:T(8,128)(2,1)S(1)}, u32[]{:S(2)}, u32[]{:S(2)}) collective-permute-start(bf16[128,192]{0,1:T(8,128)(2,1)S(1)} %convolution_convert_fusion.3), channel_id=1, source_target_pairs={{0,24},{8,0},{16,8},{24,16},{1,25},{9,1},{17,9},{25,17},{2,26},{10... | collective-permute-start | bytes 147464 | tf_op jit(solution)/shard_map/ppermute | solution.py:30
  78.1 2.2 %collective-permute-start.12 = (bf16[128,192]{0,1:T(8,128)(2,1)S(1)}, bf16[128,192]{0,1:T(8,128)(2,1)S(1)}, u32[]{:S(2)}, u32[]{:S(2)}) collective-permute-start(bf16[128,192]{0,1:T(8,128)(2,1)S(1)} %convolution_convert_fusion.2), channel_id=1, source_target_pairs={{0,16},{8,24},{16,0},{24,8},{1,17},{9,25},{17,1},{25,9},{2,18},{10... | collective-permute-start | bytes 147464 | tf_op jit(solution)/shard_map/ppermute | solution.py:30
  80.6 2.8 %collective-permute-start.13 = (bf16[128,192]{0,1:T(8,128)(2,1)S(1)}, bf16[128,192]{0,1:T(8,128)(2,1)S(1)}, u32[]{:S(2)}, u32[]{:S(2)}) collective-permute-start(bf16[128,192]{0,1:T(8,128)(2,1)S(1)} %convolution_convert_fusion.1), channel_id=1, source_target_pairs={{0,8},{8,16},{16,24},{24,0},{1,9},{9,17},{17,25},{25,1},{2,10},{10... | collective-permute-start | bytes 147464 | tf_op jit(solution)/shard_map/ppermute | solution.py:30
  83.8 1.8 %collective-permute-done.12 = bf16[128,192]{0,1:T(8,128)(2,1)S(1)} collective-permute-done((bf16[128,192]{0,1:T(8,128)(2,1)S(1)}, bf16[128,192]{0,1:T(8,128)(2,1)S(1)}, u32[]{:S(2)}, u32[]{:S(2)}) %collective-permute-start.12) | collective-permute-done | bytes 49184 | tf_op jit(solution)/shard_map/ppermute | solution.py:30
  85.6 2.2 %collective-permute-done.13 = bf16[128,192]{0,1:T(8,128)(2,1)S(1)} collective-permute-done((bf16[128,192]{0,1:T(8,128)(2,1)S(1)}, bf16[128,192]{0,1:T(8,128)(2,1)S(1)}, u32[]{:S(2)}, u32[]{:S(2)}) %collective-permute-start.13) | collective-permute-done | bytes 49184 | tf_op jit(solution)/shard_map/ppermute | solution.py:30
  88.0 1.9 %collective-permute-start.14 = (f32[2,128]{1,0:T(2,128)S(1)}, f32[2,128]{1,0:T(2,128)S(1)}, u32[]{:S(2)}, u32[]{:S(2)}) collective-permute-start(f32[2,128]{1,0:T(2,128)S(1)} %pad_maximum_fusion.1), channel_id=1, source_target_pairs={{0,1},{1,0},{2,3},{3,2},{4,5},{5,4},{6,7},{7,6},{8,9},{9,8},{10,11... | collective-permute-start | bytes 3080 | tf_op jit(solution)/shard_map/ppermute | solution.py:35
  90.0 1.1 collective-permute-done.14
  91.1 3.5 %collective-permute-start.15 = (f32[2,128]{1,0:T(2,128)S(1)}, f32[2,128]{1,0:T(2,128)S(1)}, u32[]{:S(2)}, u32[]{:S(2)}) collective-permute-start(f32[2,128]{1,0:T(2,128)S(1)} %fusion.108), channel_id=1, source_target_pairs={{0,2},{1,3},{2,4},{3,5},{4,6},{5,7},{6,0},{7,1},{8,10},{9,11},{10,... | collective-permute-start | bytes 3080 | tf_op jit(solution)/shard_map/ppermute | solution.py:30
  94.6 4.0 %collective-permute-start.16 = (f32[2,128]{1,0:T(2,128)S(1)}, f32[2,128]{1,0:T(2,128)S(1)}, u32[]{:S(2)}, u32[]{:S(2)}) collective-permute-start(f32[2,128]{1,0:T(2,128)S(1)} %fusion.108), channel_id=1, source_target_pairs={{0,4},{1,5},{2,6},{3,7},{4,0},{5,1},{6,2},{7,3},{8,12},{9,13},{10,... | collective-permute-start | bytes 3080 | tf_op jit(solution)/shard_map/ppermute | solution.py:30
  98.6 4.0 %collective-permute-start.17 = (f32[2,128]{1,0:T(2,128)S(1)}, f32[2,128]{1,0:T(2,128)S(1)}, u32[]{:S(2)}, u32[]{:S(2)}) collective-permute-start(f32[2,128]{1,0:T(2,128)S(1)} %fusion.108), channel_id=1, source_target_pairs={{0,6},{1,7},{2,0},{3,1},{4,2},{5,3},{6,4},{7,5},{8,14},{9,15},{10,... | collective-permute-start | bytes 3080 | tf_op jit(solution)/shard_map/ppermute | solution.py:30
  102.5 9.4 %all-to-all-start.1 = ((bf16[16,96,128]{2,1,0:T(8,128)(2,1)}), bf16[16,96,128]{2,1,0:T(8,128)(2,1)S(1)}, u32[]{:S(2)}, u32[]{:S(2)}) async-start(bf16[16,96,128]{2,1,0:T(8,128)(2,1)} %maximum_maximum_fusion.1), calls=%async_computation.1 | async-start | bytes 786432 | tf_op jit(solution)/shard_map/all_to_all | solution.py:21
  112.1 0.9 fusion.69
  113.0 1.2 fusion.70
  114.3 1.9 %collective-permute-start.19 = (f32[8,192]{1,0:T(8,128)S(1)}, f32[8,192]{1,0:T(8,128)S(1)}, u32[]{:S(2)}, u32[]{:S(2)}) collective-permute-start(f32[8,192]{1,0:T(8,128)S(1)} %get-tuple-element.62), channel_id=1, source_target_pairs={{0,8},{8,16},{16,24},{24,0},{1,9},{9,17},{17,25},{25,1},{2,10},{10... | collective-permute-start | bytes 18440 | tf_op jit(solution)/shard_map/ppermute | solution.py:30
  116.3 4.2 %collective-permute-start.20 = (f32[8,192]{1,0:T(8,128)S(1)}, f32[8,192]{1,0:T(8,128)S(1)}, u32[]{:S(2)}, u32[]{:S(2)}) collective-permute-start(f32[8,192]{1,0:T(8,128)S(1)} %get-tuple-element.64), channel_id=1, source_target_pairs={{0,16},{8,24},{16,0},{24,8},{1,17},{9,25},{17,1},{25,9},{2,18},{10... | collective-permute-start | bytes 18440 | tf_op jit(solution)/shard_map/ppermute | solution.py:30
  120.5 4.5 %collective-permute-start.21 = (f32[8,192]{1,0:T(8,128)S(1)}, f32[8,192]{1,0:T(8,128)S(1)}, u32[]{:S(2)}, u32[]{:S(2)}) collective-permute-start(f32[8,192]{1,0:T(8,128)S(1)} %get-tuple-element.63), channel_id=1, source_target_pairs={{0,24},{8,0},{16,8},{24,16},{1,25},{9,1},{17,9},{25,17},{2,26},{10... | collective-permute-start | bytes 18440 | tf_op jit(solution)/shard_map/ppermute | solution.py:30
  125.1 1.3 collective-permute-start.18
  126.4 4.6 %collective-permute-done.18 = bf16[30,192]{0,1:T(8,128)(2,1)S(1)} collective-permute-done((bf16[30,192]{0,1:T(8,128)(2,1)S(1)}, bf16[30,192]{0,1:T(8,128)(2,1)S(1)}, u32[]{:S(2)}, u32[]{:S(2)}) %collective-permute-start.18) | collective-permute-done | bytes 11552 | tf_op jit(solution)/shard_map/ppermute | solution.py:17
  131.1 1.8 %fusion.72 = bf16[128,192]{0,1:T(8,128)(2,1)S(1)} fusion(f32[158,192]{0,1:T(8,128)S(1)} %maximum_convert_fusion.1, f32[192]{0:T(256)S(1)} %bitcast.206, f32[192]{0:T(256)S(1)} %bitcast.208, f32[192]{0:T(256)S(1)} %bitcast.150, f32[192]{0:T(256)S(1)} %bitcast.152, f32[192]{0:T(256)S(1)} %bitcast.154, f32[192]{0:T(256)S(1)} %bitcast.156, ...), kind=kLoop, calls=%fused_computation.123 | loop fusion | flops 1523712 | bytes 3120384 | tf_op jit(solution)/shard_map/convert_element_type | solution.py:140
  132.9 0.7 fusion.19
  133.6 1.0 all-to-all-done.1
  135.2 11.0 %all-to-all-start.2 = ((bf16[16,8,192]{2,1,0:T(8,128)(2,1)}), bf16[16,8,192]{2,1,0:T(8,128)(2,1)S(1)}, u32[]{:S(2)}, u32[]{:S(2)}) async-start(bf16[16,8,192]{2,1,0:T(8,128)(2,1)} %broadcast_in_dim.9), calls=%async_computation.2 | async-start | bytes 131072 | tf_op jit(solution)/shard_map/all_to_all | solution.py:21
  147.0 12.0 %all-to-all-done.2 = bf16[16,8,192]{2,1,0:T(8,128)(2,1)S(1)} async-done(((bf16[16,8,192]{2,1,0:T(8,128)(2,1)}), bf16[16,8,192]{2,1,0:T(8,128)(2,1)S(1)}, u32[]{:S(2)}, u32[]{:S(2)}) %all-to-all-start.2) | async-done | bytes 49184 | tf_op jit(solution)/shard_map/all_to_all | solution.py:21
  159.1 3.9 %collective-permute-start.22 = (f32[8,192]{1,0:T(8,128)S(1)}, f32[8,192]{1,0:T(8,128)S(1)}, u32[]{:S(2)}, u32[]{:S(2)}) collective-permute-start(f32[8,192]{1,0:T(8,128)S(1)} %convert_reduce_fusion.2), channel_id=1, source_target_pairs={{0,24},{8,0},{16,8},{24,16},{1,25},{9,1},{17,9},{25,17},{2,26},{10... | collective-permute-start | bytes 18440 | tf_op jit(solution)/shard_map/ppermute | solution.py:30
  163.0 1.9 %collective-permute-start.23 = (f32[8,192]{1,0:T(8,128)S(1)}, f32[8,192]{1,0:T(8,128)S(1)}, u32[]{:S(2)}, u32[]{:S(2)}) collective-permute-start(f32[8,192]{1,0:T(8,128)S(1)} %convert_reduce_fusion.2), channel_id=1, source_target_pairs={{0,16},{8,24},{16,0},{24,8},{1,17},{9,25},{17,1},{25,9},{2,18},{10... | collective-permute-start | bytes 18440 | tf_op jit(solution)/shard_map/ppermute | solution.py:30
  165.0 2.8 %collective-permute-start.24 = (f32[8,192]{1,0:T(8,128)S(1)}, f32[8,192]{1,0:T(8,128)S(1)}, u32[]{:S(2)}, u32[]{:S(2)}) collective-permute-start(f32[8,192]{1,0:T(8,128)S(1)} %convert_reduce_fusion.2), channel_id=1, source_target_pairs={{0,8},{8,16},{16,24},{24,0},{1,9},{9,17},{17,25},{25,1},{2,10},{10... | collective-permute-start | bytes 18440 | tf_op jit(solution)/shard_map/ppermute | solution.py:30
  167.8 2.3 %collective-permute-done.23 = f32[8,192]{1,0:T(8,128)S(1)} collective-permute-done((f32[8,192]{1,0:T(8,128)S(1)}, f32[8,192]{1,0:T(8,128)S(1)}, u32[]{:S(2)}, u32[]{:S(2)}) %collective-permute-start.23) | collective-permute-done | bytes 6176 | tf_op jit(solution)/shard_map/ppermute | solution.py:30
  170.1 1.6 collective-permute-done.24
  (83 shorter events, 6.1 us)
Async XLA Ops:
  2.4 8.4 %copy-start = (bf16[128,192]{0,1:T(8,128)(2,1)S(1)}, bf16[128,192]{0,1:T(8,128)(2,1)}, u32[]{:S(2)}) copy-start(bf16[128,192]{0,1:T(8,128)(2,1)} %param.6) | copy-start | bytes 147460
  2.4 8.4 %copy-start.1 = (bf16[128,192]{0,1:T(8,128)(2,1)S(1)}, bf16[128,192]{0,1:T(8,128)(2,1)}, u32[]{:S(2)}) copy-start(bf16[128,192]{0,1:T(8,128)(2,1)} %param.7) | copy-start | bytes 147460
  2.4 10.1 %copy-start.4 = (f32[31,192]{1,0:T(8,128)S(1)}, f32[31,192]{1,0:T(8,128)}, u32[]{:S(2)}) copy-start(f32[31,192]{1,0:T(8,128)} %param.10) | copy-start | bytes 71428
  2.5 65.9 %collective-permute-start.5 = (bf16[128,1024]{0,1:T(8,128)(2,1)S(1)}, bf16[128,1024]{0,1:T(8,128)(2,1)S(1)}, u32[]{:S(2)}, u32[]{:S(2)}) collective-permute-start(bf16[128,1024]{0,1:T(8,128)(2,1)S(1)} %get-tuple-element.53), channel_id=1, source_target_pairs={{0,8},{8,16},{16,24},{24,0},{1,9},{9,17},{17,25},{25,1},{2,10},{10... | collective-permute-start | bytes 786440 | tf_op jit(solution)/shard_map/ppermute | solution.py:30
  6.0 62.4 %collective-permute-start.6 = (bf16[128,1024]{0,1:T(8,128)(2,1)S(1)}, bf16[128,1024]{0,1:T(8,128)(2,1)S(1)}, u32[]{:S(2)}, u32[]{:S(2)}) collective-permute-start(bf16[128,1024]{0,1:T(8,128)(2,1)S(1)} %get-tuple-element.52), channel_id=1, source_target_pairs={{0,16},{8,24},{16,0},{24,8},{1,17},{9,25},{17,1},{25,9},{2,18},{10... | collective-permute-start | bytes 786440 | tf_op jit(solution)/shard_map/ppermute | solution.py:30
  11.0 7.3 %collective-permute-start = (bf16[30,192]{0,1:T(8,128)(2,1)S(1)}, bf16[30,192]{0,1:T(8,128)(2,1)S(1)}, u32[]{:S(2)}, u32[]{:S(2)}) collective-permute-start(bf16[30,192]{0,1:T(8,128)(2,1)S(1)} %slice.520), channel_id=1, source_target_pairs={{0,8},{8,16},{16,24},{24,32},{32,40},{40,48},{48,56},{56,64},{64,7... | collective-permute-start | bytes 34568 | tf_op jit(solution)/shard_map/ppermute | solution.py:17
  18.4 3.8 %copy-start.2 = (bf16[64,192]{1,0:T(8,128)(2,1)S(1)}, bf16[64,192]{1,0:T(8,128)(2,1)}, u32[]{:S(2)}) copy-start(bf16[64,192]{1,0:T(8,128)(2,1)} %param.9) | copy-start | bytes 73732
  18.4 15.6 %slice-start = ((bf16[64,192]{1,0:T(8,128)(2,1)}), bf16[64,128]{1,0:T(8,128)(2,1)S(1)}, s32[]{:S(2)}) async-start(bf16[64,192]{1,0:T(8,128)(2,1)} %param.9), calls=%async_computation.3 | async-start | bytes 32768 | tf_op jit(solution)/shard_map/slice | solution.py:43
  20.2 34.4 %copy-start.5 = (f32[192]{0:T(256)S(1)}, f32[192]{0:T(256)}, u32[]{:S(2)}) copy-start(f32[192]{0:T(256)} %param.11) | copy-start | bytes 2308
  20.3 3.1 %collective-permute-start.1 = (f32[2,128]{1,0:T(2,128)S(1)}, f32[2,128]{1,0:T(2,128)S(1)}, u32[]{:S(2)}, u32[]{:S(2)}) collective-permute-start(f32[2,128]{1,0:T(2,128)S(1)} %pad_maximum_fusion), channel_id=1, source_target_pairs={{0,1},{1,0},{2,3},{3,2},{4,5},{5,4},{6,7},{7,6},{8,9},{9,8},{10,11... | collective-permute-start | bytes 3080 | tf_op jit(solution)/shard_map/ppermute | solution.py:35
  23.4 27.4 %collective-permute-start.2 = (f32[2,128]{1,0:T(2,128)S(1)}, f32[2,128]{1,0:T(2,128)S(1)}, u32[]{:S(2)}, u32[]{:S(2)}) collective-permute-start(f32[2,128]{1,0:T(2,128)S(1)} %fusion.109), channel_id=1, source_target_pairs={{0,2},{1,3},{2,4},{3,5},{4,6},{5,7},{6,0},{7,1},{8,10},{9,11},{10,... | collective-permute-start | bytes 3080 | tf_op jit(solution)/shard_map/ppermute | solution.py:30
  26.5 28.0 %collective-permute-start.3 = (f32[2,128]{1,0:T(2,128)S(1)}, f32[2,128]{1,0:T(2,128)S(1)}, u32[]{:S(2)}, u32[]{:S(2)}) collective-permute-start(f32[2,128]{1,0:T(2,128)S(1)} %fusion.109), channel_id=1, source_target_pairs={{0,4},{1,5},{2,6},{3,7},{4,0},{5,1},{6,2},{7,3},{8,12},{9,13},{10,... | collective-permute-start | bytes 3080 | tf_op jit(solution)/shard_map/ppermute | solution.py:30
  29.4 25.1 %collective-permute-start.4 = (f32[2,128]{1,0:T(2,128)S(1)}, f32[2,128]{1,0:T(2,128)S(1)}, u32[]{:S(2)}, u32[]{:S(2)}) collective-permute-start(f32[2,128]{1,0:T(2,128)S(1)} %fusion.109), channel_id=1, source_target_pairs={{0,6},{1,7},{2,0},{3,1},{4,2},{5,3},{6,4},{7,5},{8,14},{9,15},{10,... | collective-permute-start | bytes 3080 | tf_op jit(solution)/shard_map/ppermute | solution.py:30
  34.8 38.6 %all-to-all-start = ((bf16[16,96,128]{2,1,0:T(8,128)(2,1)}), bf16[16,96,128]{2,1,0:T(8,128)(2,1)S(1)}, u32[]{:S(2)}, u32[]{:S(2)}) async-start(bf16[16,96,128]{2,1,0:T(8,128)(2,1)} %broadcast_in_dim.8), calls=%async_computation | async-start | bytes 786432 | tf_op jit(solution)/shard_map/all_to_all | solution.py:21
  50.8 17.7 %collective-permute-start.7 = (bf16[128,1024]{0,1:T(8,128)(2,1)S(1)}, bf16[128,1024]{0,1:T(8,128)(2,1)S(1)}, u32[]{:S(2)}, u32[]{:S(2)}) collective-permute-start(bf16[128,1024]{0,1:T(8,128)(2,1)S(1)} %get-tuple-element.51), channel_id=1, source_target_pairs={{0,24},{8,0},{16,8},{24,16},{1,25},{9,1},{17,9},{25,17},{2,26},{10... | collective-permute-start | bytes 786440 | tf_op jit(solution)/shard_map/ppermute | solution.py:30
  54.7 6.3 %collective-permute-start.10 = (bf16[128,192]{0,1:T(8,128)(2,1)S(1)}, bf16[128,192]{0,1:T(8,128)(2,1)S(1)}, u32[]{:S(2)}, u32[]{:S(2)}) collective-permute-start(bf16[128,192]{0,1:T(8,128)(2,1)S(1)} %fusion.32), channel_id=1, source_target_pairs={{0,24},{8,0},{16,8},{24,16},{1,25},{9,1},{17,9},{25,17},{2,26},{10... | collective-permute-start | bytes 147464 | tf_op jit(solution)/shard_map/ppermute | solution.py:30
  57.0 7.5 %collective-permute-start.8 = (bf16[128,192]{0,1:T(8,128)(2,1)S(1)}, bf16[128,192]{0,1:T(8,128)(2,1)S(1)}, u32[]{:S(2)}, u32[]{:S(2)}) collective-permute-start(bf16[128,192]{0,1:T(8,128)(2,1)S(1)} %fusion.32), channel_id=1, source_target_pairs={{0,8},{8,16},{16,24},{24,0},{1,9},{9,17},{17,25},{25,1},{2,10},{10... | collective-permute-start | bytes 147464 | tf_op jit(solution)/shard_map/ppermute | solution.py:30
  61.0 7.5 %collective-permute-start.9 = (bf16[128,192]{0,1:T(8,128)(2,1)S(1)}, bf16[128,192]{0,1:T(8,128)(2,1)S(1)}, u32[]{:S(2)}, u32[]{:S(2)}) collective-permute-start(bf16[128,192]{0,1:T(8,128)(2,1)S(1)} %fusion.32), channel_id=1, source_target_pairs={{0,16},{8,24},{16,0},{24,8},{1,17},{9,25},{17,1},{25,9},{2,18},{10... | collective-permute-start | bytes 147464 | tf_op jit(solution)/shard_map/ppermute | solution.py:30
  74.0 9.8 %collective-permute-start.11 = (bf16[128,192]{0,1:T(8,128)(2,1)S(1)}, bf16[128,192]{0,1:T(8,128)(2,1)S(1)}, u32[]{:S(2)}, u32[]{:S(2)}) collective-permute-start(bf16[128,192]{0,1:T(8,128)(2,1)S(1)} %convolution_convert_fusion.3), channel_id=1, source_target_pairs={{0,24},{8,0},{16,8},{24,16},{1,25},{9,1},{17,9},{25,17},{2,26},{10... | collective-permute-start | bytes 147464 | tf_op jit(solution)/shard_map/ppermute | solution.py:30
  78.1 7.5 %collective-permute-start.12 = (bf16[128,192]{0,1:T(8,128)(2,1)S(1)}, bf16[128,192]{0,1:T(8,128)(2,1)S(1)}, u32[]{:S(2)}, u32[]{:S(2)}) collective-permute-start(bf16[128,192]{0,1:T(8,128)(2,1)S(1)} %convolution_convert_fusion.2), channel_id=1, source_target_pairs={{0,16},{8,24},{16,0},{24,8},{1,17},{9,25},{17,1},{25,9},{2,18},{10... | collective-permute-start | bytes 147464 | tf_op jit(solution)/shard_map/ppermute | solution.py:30
  80.6 7.2 %collective-permute-start.13 = (bf16[128,192]{0,1:T(8,128)(2,1)S(1)}, bf16[128,192]{0,1:T(8,128)(2,1)S(1)}, u32[]{:S(2)}, u32[]{:S(2)}) collective-permute-start(bf16[128,192]{0,1:T(8,128)(2,1)S(1)} %convolution_convert_fusion.1), channel_id=1, source_target_pairs={{0,8},{8,16},{16,24},{24,0},{1,9},{9,17},{17,25},{25,1},{2,10},{10... | collective-permute-start | bytes 147464 | tf_op jit(solution)/shard_map/ppermute | solution.py:30
  88.0 3.1 %collective-permute-start.14 = (f32[2,128]{1,0:T(2,128)S(1)}, f32[2,128]{1,0:T(2,128)S(1)}, u32[]{:S(2)}, u32[]{:S(2)}) collective-permute-start(f32[2,128]{1,0:T(2,128)S(1)} %pad_maximum_fusion.1), channel_id=1, source_target_pairs={{0,1},{1,0},{2,3},{3,2},{4,5},{5,4},{6,7},{7,6},{8,9},{9,8},{10,11... | collective-permute-start | bytes 3080 | tf_op jit(solution)/shard_map/ppermute | solution.py:35
  91.1 20.8 %collective-permute-start.15 = (f32[2,128]{1,0:T(2,128)S(1)}, f32[2,128]{1,0:T(2,128)S(1)}, u32[]{:S(2)}, u32[]{:S(2)}) collective-permute-start(f32[2,128]{1,0:T(2,128)S(1)} %fusion.108), channel_id=1, source_target_pairs={{0,2},{1,3},{2,4},{3,5},{4,6},{5,7},{6,0},{7,1},{8,10},{9,11},{10,... | collective-permute-start | bytes 3080 | tf_op jit(solution)/shard_map/ppermute | solution.py:30
  94.6 17.4 %collective-permute-start.16 = (f32[2,128]{1,0:T(2,128)S(1)}, f32[2,128]{1,0:T(2,128)S(1)}, u32[]{:S(2)}, u32[]{:S(2)}) collective-permute-start(f32[2,128]{1,0:T(2,128)S(1)} %fusion.108), channel_id=1, source_target_pairs={{0,4},{1,5},{2,6},{3,7},{4,0},{5,1},{6,2},{7,3},{8,12},{9,13},{10,... | collective-permute-start | bytes 3080 | tf_op jit(solution)/shard_map/ppermute | solution.py:30
  98.6 13.4 %collective-permute-start.17 = (f32[2,128]{1,0:T(2,128)S(1)}, f32[2,128]{1,0:T(2,128)S(1)}, u32[]{:S(2)}, u32[]{:S(2)}) collective-permute-start(f32[2,128]{1,0:T(2,128)S(1)} %fusion.108), channel_id=1, source_target_pairs={{0,6},{1,7},{2,0},{3,1},{4,2},{5,3},{6,4},{7,5},{8,14},{9,15},{10,... | collective-permute-start | bytes 3080 | tf_op jit(solution)/shard_map/ppermute | solution.py:30
  102.5 32.1 %all-to-all-start.1 = ((bf16[16,96,128]{2,1,0:T(8,128)(2,1)}), bf16[16,96,128]{2,1,0:T(8,128)(2,1)S(1)}, u32[]{:S(2)}, u32[]{:S(2)}) async-start(bf16[16,96,128]{2,1,0:T(8,128)(2,1)} %maximum_maximum_fusion.1), calls=%async_computation.1 | async-start | bytes 786432 | tf_op jit(solution)/shard_map/all_to_all | solution.py:21
  114.3 12.0 %collective-permute-start.19 = (f32[8,192]{1,0:T(8,128)S(1)}, f32[8,192]{1,0:T(8,128)S(1)}, u32[]{:S(2)}, u32[]{:S(2)}) collective-permute-start(f32[8,192]{1,0:T(8,128)S(1)} %get-tuple-element.62), channel_id=1, source_target_pairs={{0,8},{8,16},{16,24},{24,0},{1,9},{9,17},{17,25},{25,1},{2,10},{10... | collective-permute-start | bytes 18440 | tf_op jit(solution)/shard_map/ppermute | solution.py:30
  116.3 10.1 %collective-permute-start.20 = (f32[8,192]{1,0:T(8,128)S(1)}, f32[8,192]{1,0:T(8,128)S(1)}, u32[]{:S(2)}, u32[]{:S(2)}) collective-permute-start(f32[8,192]{1,0:T(8,128)S(1)} %get-tuple-element.64), channel_id=1, source_target_pairs={{0,16},{8,24},{16,0},{24,8},{1,17},{9,25},{17,1},{25,9},{2,18},{10... | collective-permute-start | bytes 18440 | tf_op jit(solution)/shard_map/ppermute | solution.py:30
  120.5 5.9 %collective-permute-start.21 = (f32[8,192]{1,0:T(8,128)S(1)}, f32[8,192]{1,0:T(8,128)S(1)}, u32[]{:S(2)}, u32[]{:S(2)}) collective-permute-start(f32[8,192]{1,0:T(8,128)S(1)} %get-tuple-element.63), channel_id=1, source_target_pairs={{0,24},{8,0},{16,8},{24,16},{1,25},{9,1},{17,9},{25,17},{2,26},{10... | collective-permute-start | bytes 18440 | tf_op jit(solution)/shard_map/ppermute | solution.py:30
  125.1 6.0 %collective-permute-start.18 = (bf16[30,192]{0,1:T(8,128)(2,1)S(1)}, bf16[30,192]{0,1:T(8,128)(2,1)S(1)}, u32[]{:S(2)}, u32[]{:S(2)}) collective-permute-start(bf16[30,192]{0,1:T(8,128)(2,1)S(1)} %bitcast.143), channel_id=1, source_target_pairs={{8,0},{16,8},{24,16},{32,24},{40,32},{48,40},{56,48},{64,56},{72,6... | collective-permute-start | bytes 34568 | tf_op jit(solution)/shard_map/ppermute | solution.py:17
  135.2 23.8 %all-to-all-start.2 = ((bf16[16,8,192]{2,1,0:T(8,128)(2,1)}), bf16[16,8,192]{2,1,0:T(8,128)(2,1)S(1)}, u32[]{:S(2)}, u32[]{:S(2)}) async-start(bf16[16,8,192]{2,1,0:T(8,128)(2,1)} %broadcast_in_dim.9), calls=%async_computation.2 | async-start | bytes 131072 | tf_op jit(solution)/shard_map/all_to_all | solution.py:21
  159.1 8.7 %collective-permute-start.22 = (f32[8,192]{1,0:T(8,128)S(1)}, f32[8,192]{1,0:T(8,128)S(1)}, u32[]{:S(2)}, u32[]{:S(2)}) collective-permute-start(f32[8,192]{1,0:T(8,128)S(1)} %convert_reduce_fusion.2), channel_id=1, source_target_pairs={{0,24},{8,0},{16,8},{24,16},{1,25},{9,1},{17,9},{25,17},{2,26},{10... | collective-permute-start | bytes 18440 | tf_op jit(solution)/shard_map/ppermute | solution.py:30
  163.0 7.0 %collective-permute-start.23 = (f32[8,192]{1,0:T(8,128)S(1)}, f32[8,192]{1,0:T(8,128)S(1)}, u32[]{:S(2)}, u32[]{:S(2)}) collective-permute-start(f32[8,192]{1,0:T(8,128)S(1)} %convert_reduce_fusion.2), channel_id=1, source_target_pairs={{0,16},{8,24},{16,0},{24,8},{1,17},{9,25},{17,1},{25,9},{2,18},{10... | collective-permute-start | bytes 18440 | tf_op jit(solution)/shard_map/ppermute | solution.py:30
  165.0 6.8 %collective-permute-start.24 = (f32[8,192]{1,0:T(8,128)S(1)}, f32[8,192]{1,0:T(8,128)S(1)}, u32[]{:S(2)}, u32[]{:S(2)}) collective-permute-start(f32[8,192]{1,0:T(8,128)S(1)} %convert_reduce_fusion.2), channel_id=1, source_target_pairs={{0,8},{8,16},{16,24},{24,0},{1,9},{9,17},{17,25},{25,1},{2,10},{10... | collective-permute-start | bytes 18440 | tf_op jit(solution)/shard_map/ppermute | solution.py:30
  171.8 0.6 copy-start.3
